TPU v7x, 256 devices: a whole 4x4x8 slice. The times are simulated.
256 devices in a mesh: ep: 64 (over z, y, core), tp: 4 (over x).
Axes of the slice: x: 4, y: 4, z: 8, core: 2. Of those that a mesh axis runs over, the one named last changes fastest.
Arguments:
- outer_gate: bfloat16 [32768, 2048], P('ep', 'tp'), may hold values from -6 to 6
- inner_gate: bfloat16 [32768, 2048], P('ep', 'tp'), may hold values from -6 to 6
- conv_values: bfloat16 [32768, 2048], P('ep', 'tp'), may hold values from -6 to 6
- conv_taps: bfloat16 [3, 2048], P(None, 'tp'), may hold values from -3 to 3
- out_weight: bfloat16 [2048, 2048], P('tp'), may hold values from -0.125 to 0.125
- moe_input: bfloat16 [32768, 2048], P(('ep', 'tp')), may hold values from -6 to 6
- norm_gain: bfloat16 [2048], replicated, may hold values from 0.099609375 to 1.8984375
- gate_proj: bfloat16 [64, 2048, 1024], P('ep', None, 'tp'), may hold values from -0.125 to 0.125
- up_proj: bfloat16 [64, 2048, 1024], P('ep', None, 'tp'), may hold values from -0.125 to 0.125
- down_proj: bfloat16 [64, 1024, 2048], P('ep', 'tp'), may hold values from -0.1875 to 0.1875
- shared_gate: bfloat16 [2048, 1024], P(None, 'tp'), may hold values from -0.125 to 0.125
- shared_up: bfloat16 [2048, 1024], P(None, 'tp'), may hold values from -0.125 to 0.125
- shared_down: bfloat16 [1024, 2048], P('tp'), may hold values from -0.1875 to 0.1875
- routes: int32 [32768, 2], P('ep'), may hold values from 0 to 63, all different within a row; in each aligned block of 128 rows (0 to 127, 128 to 255, ...) at most 8 rows name the same one
- route_weight: float32 [32768, 2], P('ep'), may hold values from 0.3 to 1.5
Outputs:
- mixer_out: bfloat16 [32768, 2048], P(('ep', 'tp'))
- expert_mix: bfloat16 [32768, 2048], P(('ep', 'tp'))
Inputs may be any that keep to these rules, and one draw needn't show every extreme that they name: `routes`: each row names 2 different experts. In the 128 rows of one device no expert is named more than 8 times, and in every draw some expert is named exactly 8 times in one device's rows.
All inputs are finite; a program needn't handle non-finite values.
Results may differ from a plain program's by a relative error of at most 0.012.
Values may be sent and summed in bfloat16 or wider, within the bound.
A program may use at most 128 MiB of HBM per device.

v0:
```python
from functools import partial
import jax
import jax.numpy as jnp
from jax import lax
from jax.sharding import PartitionSpec as P

epsilon = 1e-06


def shifted(block, axis, distance):
    devices = range(lax.axis_size(axis))
    route = [(i - distance, i) for i in devices if i - distance in devices]
    return lax.ppermute(block, axis, route)


def from_everyone(array, axis):
    length = lax.axis_size(axis)
    return lax.all_to_all(
        jnp.broadcast_to(array[None], (length, *array.shape)), axis, 0, 0, tiled=True
    )


def joined_along(blocks, dim):
    shape = list(blocks.shape[1:])
    shape[dim] *= blocks.shape[0]
    return jnp.moveaxis(blocks, 0, dim).reshape(shape)


def collect(array, axis, dim):
    blocks = from_everyone(array, axis)
    return joined_along(blocks, dim)


def gather_turned(arrays, axis, dims):
    turned = [jnp.moveaxis(a, dim, 0) for a, dim in zip(arrays, dims)]
    both = jnp.concatenate([t.reshape(len(t), -1) for t in turned], axis=1)
    result, at, outs = (lax.all_gather(both, axis, axis=0, tiled=True), 0, [])
    for t, dim in zip(turned, dims):
        share = result[:, at : at + t[0].size].reshape(-1, *t.shape[1:])
        outs.append(jnp.moveaxis(share, 0, dim))
        at += t[0].size
    return tuple(outs)


def rms_norm(inputs, scales):
    values = inputs.astype(jnp.float32)
    square = jnp.mean(values * values, axis=-1, keepdims=True)
    return (values * lax.rsqrt(square + epsilon) * scales.astype(jnp.float32)).astype(jnp.bfloat16)


def swiglu(inputs, gate_w, up_w):
    gate_term = jnp.dot(inputs, gate_w, preferred_element_type=jnp.float32)
    upward = jnp.dot(inputs, up_w, preferred_element_type=jnp.float32)
    return (jax.nn.silu(gate_term) * upward).astype(jnp.bfloat16)


def slot_table(block_routes, experts, capacity):
    flat_ids = block_routes.reshape(-1)
    onehot = (flat_ids[:, None] == jnp.arange(experts, dtype=jnp.int32)[None, :]).astype(jnp.int32)
    earlier = jnp.cumsum(onehot, axis=0) - onehot
    slot_ids = jnp.sum(earlier * onehot, axis=1)
    targets = flat_ids * capacity + slot_ids
    owners = jnp.arange(flat_ids.shape[0], dtype=jnp.int32) // block_routes.shape[1]
    sources = jnp.zeros((experts * capacity,), jnp.int32).at[targets].set(owners)
    filled = jnp.zeros((experts * capacity,), jnp.bfloat16).at[targets].set(1.0)
    return (sources, filled, targets)


def send_own(normed, own_routes, table_maker, ep_count, capacity):
    sources, filled, own_targets = table_maker(own_routes)
    outgoing = (normed[sources] * filled[:, None]).reshape(ep_count, capacity, normed.shape[1])
    landed = lax.all_to_all(outgoing, "ep", split_axis=0, concat_axis=0, tiled=True)
    return (landed, own_targets)


def per_device(
    outer_gate,
    inner_gate,
    conv_values,
    conv_taps,
    out_weight,
    moe_input,
    norm_gain,
    gate_proj,
    up_proj,
    down_proj,
    shared_gate,
    shared_up,
    shared_down,
    routes,
    route_weight,
):
    tp_count = lax.axis_size("tp")
    ep_count = lax.axis_size("ep")
    my_slot = lax.axis_index("tp")
    group_len = inner_gate.shape[0]
    mix_rows = group_len // tp_count
    channels = inner_gate.shape[1]
    model_width = moe_input.shape[1]
    own_rows = moe_input.shape[0]
    top_count = routes.shape[1]
    capacity = 2 * own_rows * top_count // ep_count
    slot_rows = ep_count * capacity
    reach_rows = conv_taps.shape[0] - 1
    edge_rows = jnp.stack(
        (inner_gate[group_len - reach_rows :], conv_values[group_len - reach_rows :])
    )
    before = shifted(edge_rows, "ep", 1)
    full_gate = jnp.concatenate((before[0], inner_gate), axis=0).astype(jnp.float32)
    full_values = jnp.concatenate((before[1], conv_values), axis=0).astype(jnp.float32)
    product = full_gate * full_values
    tap_values = conv_taps.astype(jnp.float32)
    convolved = tap_values[0] * product[0:group_len]
    for offset in range(1, reach_rows + 1):
        convolved = convolved + tap_values[offset] * product[offset : offset + group_len]
    gate_rows = (outer_gate.astype(jnp.float32) * convolved).astype(jnp.bfloat16)
    gate_rows = gate_rows.reshape(tp_count, mix_rows, channels)
    normed = rms_norm(moe_input, norm_gain)
    group_normed = collect(normed, "tp", 0)
    group_split = group_normed.reshape(tp_count, own_rows, model_width)
    own_weights = lax.dynamic_slice_in_dim(route_weight, my_slot * own_rows, own_rows, 0)
    own_routes = lax.dynamic_slice_in_dim(routes, my_slot * own_rows, own_rows, 0)
    table_maker = partial(slot_table, experts=ep_count, capacity=capacity)
    local_routed = None
    landed, own_targets = send_own(normed, own_routes, table_maker, ep_count, capacity)
    gate_full, up_full, down_full = gather_turned((gate_proj, up_proj, down_proj), "tp", (2, 2, 1))
    hidden = swiglu(landed.reshape(slot_rows, model_width), gate_full[0], up_full[0])
    unit_block = hidden.shape[1] // tp_count
    local_routed = jnp.zeros((slot_rows, model_width), jnp.float32)
    for piece_idx in range(tp_count):
        partial_sum = jnp.dot(
            hidden[:, piece_idx * unit_block : (piece_idx + 1) * unit_block],
            down_full[0, piece_idx * unit_block : (piece_idx + 1) * unit_block],
            preferred_element_type=jnp.float32,
        ).astype(jnp.bfloat16)
        local_routed = local_routed + partial_sum.astype(jnp.float32)
    routed_rows = 0
    expert_block = routed_rows + own_rows
    joint_block = mix_rows + expert_block
    dev_count = joint_block * lax.axis_size("tp") // joint_block
    block_rows = gate_rows
    block_rows = block_rows.reshape(dev_count * mix_rows, channels)
    projected = jnp.dot(block_rows, out_weight, preferred_element_type=jnp.float32)
    shared_in = group_split
    shared_in = shared_in.reshape(dev_count * own_rows, model_width)
    shared_out = jnp.dot(
        swiglu(shared_in, shared_gate, shared_up), shared_down, preferred_element_type=jnp.float32
    )
    shared_out = shared_out.reshape(dev_count, own_rows, model_width)
    combined = jnp.concatenate(
        (projected.reshape(dev_count, mix_rows, model_width), shared_out), axis=1
    )
    summed = lax.psum_scatter(
        combined.reshape(dev_count * joint_block, model_width).astype(jnp.bfloat16),
        "tp",
        scatter_dimension=0,
        tiled=True,
    ).astype(jnp.float32)
    mixer_out = summed[:mix_rows].astype(jnp.bfloat16)
    expert_total = summed[mix_rows:]
    routed_back = local_routed.astype(jnp.bfloat16)
    routed_back = routed_back.reshape(ep_count, capacity, model_width)
    returned = lax.all_to_all(routed_back, "ep", split_axis=0, concat_axis=0, tiled=True).reshape(
        slot_rows, model_width
    )
    picked = returned[own_targets].reshape(own_rows, top_count, model_width).astype(jnp.float32)
    routed = jnp.sum(picked * own_weights[:, :, None], axis=1)
    expert_mix = (expert_total + routed).astype(jnp.bfloat16)
    return (mixer_out, expert_mix)


def solution(mesh):
    return jax.shard_map(
        per_device,
        mesh=mesh,
        in_specs=(
            P("ep", "tp"),
            P("ep", "tp"),
            P("ep", "tp"),
            P(None, "tp"),
            P("tp", None),
            P(("ep", "tp"), None),
            P(),
            P("ep", None, "tp"),
            P("ep", None, "tp"),
            P("ep", "tp", None),
            P(None, "tp"),
            P(None, "tp"),
            P("tp", None),
            P("ep", None),
            P("ep", None),
        ),
        out_specs=(P(("ep", "tp"), None), P(("ep", "tp"), None)),
        check_vma=False,
    )
```

profile of v0, /device:TPU:8, one launch (start us, length us, event | category | flops | bytes accessed | tf_op | source)
XLA Modules:
  0.0 245.1 jit_solution(8007941486165297258)
XLA Ops:
  7.2 0.0 copy-start
  7.2 0.0 all-gather.2.cloned.1.call-start
  7.2 1.6 copy.24
  8.9 2.3 copy.25
  11.1 3.0 %pad_maximum_fusion.1 = bf16[256,6144]{1,0:T(8,128)(2,1)} fusion(bf16[256,2048]{1,0:T(8,128)(2,1)} %bitcast.97, bf16[256,2048]{1,0:T(8,128)(2,1)} %bitcast.94, bf16[256,2048]{1,0:T(8,128)(2,1)S(1)} %bitcast.93), kind=kLoop, calls=%fused_computation.11 | loop fusion | flops 9437184 | bytes 6291456 | tf_op jit(solution)/shard_map/concatenate | solution.py:36
  14.1 0.0 all-gather.2.cloned.1.call-update
  14.1 0.7 copy-done.9
  14.8 0.4 copy-done.2
  15.2 0.2 fusion.8
  15.4 0.2 fusion.10
  15.6 1.6 broadcast_in_dim.8
  17.2 4.5 %all-to-all-start = ((bf16[4,128,2048]{2,1,0:T(8,128)(2,1)}), bf16[4,128,2048]{2,1,0:T(8,128)(2,1)}, u32[]{:S(2)}, u32[]{:S(2)}) async-start(bf16[4,128,2048]{2,1,0:T(8,128)(2,1)} %broadcast_in_dim.8), calls=%async_computation | async-start | bytes 4194304 | tf_op jit(solution)/shard_map/all_to_all | solution.py:18
  21.7 0.7 broadcast_multiply_fusion
  22.3 0.1 copy.21
  22.5 0.1 eq.29
  22.6 0.1 eq.25
  22.8 0.6 reduce-window.6
  23.4 0.2 slice_reduce_fusion
  23.6 0.1 copy.20
  23.7 0.1 mul.132
  23.9 0.1 fusion.31
  24.0 1.4 scatter_custom_fusion
  25.4 3.3 %gather_fusion = bf16[512,2048]{1,0:T(8,128)(2,1)} fusion(bf16[128,2048]{1,0:T(8,128)(2,1)S(1)} %fusion.10, s32[1024]{0:T(1024)S(1)} %pad_clamp_fusion.1), kind=kCustom, calls=%fused_computation | custom fusion | bytes 4196352 | tf_op jit(solution)/shard_map/gather | solution.py:71
  28.7 2.2 scatter_custom_fusion.1
  30.9 0.1 mul.134
  31.0 3.5 %bitcast_multiply_fusion = bf16[64,8,2048]{2,1,0:T(8,128)(2,1)} fusion(bf16[512,2048]{1,0:T(8,128)(2,1)} %gather_fusion, bf16[64,8]{1,0:T(8,128)(2,1)S(1)} %mul.134), kind=kLoop, calls=%fused_computation.21 | loop fusion | flops 1048576 | bytes 4195328 | tf_op jit(solution)/shard_map/mul | solution.py:71
  34.5 26.7 %all-to-all-done = bf16[4,128,2048]{2,1,0:T(8,128)(2,1)} async-done(((bf16[4,128,2048]{2,1,0:T(8,128)(2,1)}), bf16[4,128,2048]{2,1,0:T(8,128)(2,1)}, u32[]{:S(2)}, u32[]{:S(2)}) %all-to-all-start) | async-done | bytes 2097184 | tf_op jit(solution)/shard_map/all_to_all | solution.py:18
  61.2 13.8 %all-to-all-start.1 = ((bf16[64,8,2048]{2,1,0:T(8,128)(2,1)}), bf16[64,8,2048]{2,1,0:T(8,128)(2,1)}, u32[]{:S(2)}, u32[]{:S(2)}) async-start(bf16[64,8,2048]{2,1,0:T(8,128)(2,1)} %bitcast_multiply_fusion), calls=%async_computation.2 | async-start | bytes 4194304 | tf_op jit(solution)/shard_map/all_to_all | solution.py:72
  75.0 0.0 reduce-scatter.2.cloned.1.call-start
  75.0 0.0 copy-done.6
  75.1 0.0 copy-done.7
  75.1 0.0 copy-start.12
  75.1 2.3 collective-permute-start
  77.5 0.0 copy-done.8
  77.5 3.1 %collective-permute-done = bf16[2,2,512]{2,1,0:T(2,128)(2,1)S(1)} collective-permute-done((bf16[2,2,512]{2,1,0:T(2,128)(2,1)S(1)}, bf16[2,2,512]{2,1,0:T(2,128)(2,1)S(1)}, u32[]{:S(2)}, u32[]{:S(2)}) %collective-permute-start) | collective-permute-done | bytes 4128 | tf_op jit(solution)/shard_map/ppermute | solution.py:13
  80.6 0.2 convert_multiply_fusion.2
  80.9 0.0 copy-start.10
  80.9 2.8 %convolution_convert_fusion.5 = bf16[512,2048]{1,0:T(8,128)(2,1)} fusion(bf16[512,2048]{1,0:T(8,128)(2,1)S(1)} %copy-done, f32[514,512]{1,0:T(8,128)S(1)} %convert_multiply_fusion.2, bf16[512,512]{1,0:T(8,128)(2,1)S(1)} %copy-done.12, f32[512]{0:T(512)S(1)} %bitcast.104, f32[512]{0:T(512)S(1)} %bitcast.103, f32[512]{0:T(512)S(1)} %bitcast.102), kind=kOutput, calls=%fused_computation.17 | convolution fusion | flops 1076887552 | bytes 7870464 | tf_op jit(solution)/shard_map/dot_general | solution.py:143
  83.6 3.2 %fusion.39 = f32[512,256]{1,0:T(8,128)} fusion(bf16[512,2048]{1,0:T(8,128)(2,1)} %bitcast.8, bf16[2048,256]{1,0:T(8,128)(2,1)S(1)} %copy-done.10), kind=kOutput, calls=%fused_computation.89 | convolution fusion | flops 536870912 | bytes 3670016 | tf_op jit(solution)/shard_map/dot_general | solution.py:52
  86.9 0.0 copy-done.11
  86.9 5.8 %convolution_convert_fusion.4 = bf16[512,2048]{1,0:T(8,128)(2,1)} fusion(bf16[256,2048]{1,0:T(8,128)(2,1)S(1)} %copy-done.11, bf16[512,2048]{1,0:T(8,128)(2,1)} %bitcast.8, bf16[2048,256]{1,0:T(8,128)(2,1)} %param.26, f32[512,256]{1,0:T(8,128)} %fusion.39), kind=kOutput, calls=%fused_computation.16 | convolution fusion | flops 1075576832 | bytes 6815744 | tf_op jit(solution)/shard_map/dot_general | solution.py:146
  92.7 4.2 %pad_maximum_fusion = bf16[4,256,2048]{2,1,0:T(8,128)(2,1)} fusion(bf16[4,128,2048]{2,1,0:T(8,128)(2,1)} %bitcast.96, bf16[4,128,2048]{2,1,0:T(8,128)(2,1)S(1)} %bitcast.95), kind=kLoop, calls=%fused_computation.9 | loop fusion | flops 8388608 | bytes 8388608 | tf_op jit(solution)/shard_map/concatenate | solution.py:150
  96.9 0.0 reduce-scatter.2.cloned.1.call-update
  96.9 29.3 %all-to-all-done.1 = bf16[64,8,2048]{2,1,0:T(8,128)(2,1)} async-done(((bf16[64,8,2048]{2,1,0:T(8,128)(2,1)}), bf16[64,8,2048]{2,1,0:T(8,128)(2,1)}, u32[]{:S(2)}, u32[]{:S(2)}) %all-to-all-start.1) | async-done | bytes 2097184 | tf_op jit(solution)/shard_map/all_to_all | solution.py:72
  126.1 23.3 %all-gather.2.cloned.1.call-done = bf16[1024,6144]{1,0:T(8,128)(2,1)} async-done(((bf16[256,6144]{1,0:T(8,128)(2,1)}), bf16[1024,6144]{1,0:T(8,128)(2,1)}) %all-gather.2.cloned.1.call-update) | async-done | bytes 12582928 | tf_op jit(solution)/shard_map/all_gather | solution.py:37
  149.4 5.3 %fusion.1 = f32[512,1024]{1,0:T(8,128)S(1)} fusion(bf16[1024,6144]{1,0:T(8,128)(2,1)} %all-gather.2.cloned.1.call-done, bf16[64,8,2048]{2,1,0:T(8,128)(2,1)} %all-to-all-done.1), kind=kOutput, calls=%fused_computation.8 | convolution fusion | flops 2147483648 | bytes 8388608 | tf_op jit(solution)/shard_map/dot_general | solution.py:52
  154.7 1.1 copy-done.4
  155.8 0.6 slice_bitcast_fusion
  156.4 4.1 %multiply_convert_fusion = bf16[512,1024]{1,0:T(8,128)(2,1)S(1)} fusion(f32[512,1024]{1,0:T(8,128)S(1)} %fusion.1, bf16[1024,6144]{1,0:T(8,128)(2,1)S(1)} %copy-done.4, bf16[64,8,2048]{2,1,0:T(8,128)(2,1)} %all-to-all-done.1), kind=kOutput, calls=%fused_computation.23 | convolution fusion | flops 2150629376 | bytes 9437184 | tf_op jit(solution)/shard_map/dot_general | solution.py:53
  160.5 0.7 convolution_convert_fusion.2
  161.3 0.7 convolution_convert_fusion.1
  162.0 0.7 convolution_convert_fusion
  162.7 2.6 %fusion.2 = bf16[64,8,2048]{2,1,0:T(8,128)(2,1)} fusion(bf16[512,2048]{1,0:T(8,128)(2,1)S(1)} %convolution_convert_fusion, bf16[512,2048]{1,0:T(8,128)(2,1)S(1)} %convolution_convert_fusion.1, bf16[512,2048]{1,0:T(8,128)(2,1)S(1)} %convolution_convert_fusion.2, bf16[1,1024,2048]{2,1,0:T(8,128)(2,1)S(1)} %slice_bitcast_fusion, ...), kind=kOutput, calls=%fused_computation.18 | convolution fusion | flops 546308096 | bytes 9699328 | tf_op jit(solution)/shard_map/dot_general | solution.py:131
  165.4 12.1 %all-to-all-start.2 = ((bf16[64,8,2048]{2,1,0:T(8,128)(2,1)}), bf16[64,8,2048]{2,1,0:T(8,128)(2,1)S(1)}, u32[]{:S(2)}, u32[]{:S(2)}) async-start(bf16[64,8,2048]{2,1,0:T(8,128)(2,1)} %fusion.2), calls=%async_computation.3 | async-start | bytes 4194304 | tf_op jit(solution)/shard_map/all_to_all | solution.py:163
  177.5 0.7 constant_dynamic-slice_fusion
  178.1 0.1 copy.26
  178.3 24.4 %reduce-scatter.2.cloned.1.call-done = bf16[256,2048]{1,0:T(8,128)(2,1)} async-done(((bf16[1024,2048]{1,0:T(8,128)(2,1)}), bf16[256,2048]{1,0:T(8,128)(2,1)}) %reduce-scatter.2.cloned.1.call-update) | async-done | bytes 1048592 | tf_op jit(solution)/shard_map/reduce_scatter | solution.py:153
  202.7 1.9 slice.117
  204.5 24.2 %all-to-all-done.2 = bf16[64,8,2048]{2,1,0:T(8,128)(2,1)S(1)} async-done(((bf16[64,8,2048]{2,1,0:T(8,128)(2,1)}), bf16[64,8,2048]{2,1,0:T(8,128)(2,1)S(1)}, u32[]{:S(2)}, u32[]{:S(2)}) %all-to-all-start.2) | async-done | bytes 2097184 | tf_op jit(solution)/shard_map/all_to_all | solution.py:163
  228.7 1.4 gather_fusion.1
  230.1 0.0 copy-start.1
  230.1 2.4 reshape.113
  232.4 4.9 %multiply_reduce_fusion = f32[128,2048]{1,0:T(8,128)S(1)} fusion(f32[128,2,2048]{2,1,0:T(2,128)} %reshape.113, f32[128,2]{1,0:T(8,128)S(1)} %copy.26), kind=kLoop, calls=%fused_computation.22 | loop fusion | flops 786432 | bytes 3146752 | tf_op jit(solution)/shard_map/reduce_sum | solution.py:167
  237.3 0.9 add_convert_fusion.1
  (30 shorter events, 0.2 us)
Async XLA Ops:
  7.2 73.7 %copy-start = (bf16[512,2048]{1,0:T(8,128)(2,1)S(1)}, bf16[512,2048]{1,0:T(8,128)(2,1)}, u32[]{:S(2)}) copy-start(bf16[512,2048]{1,0:T(8,128)(2,1)} %param.19) | copy-start | bytes 6291460
  7.2 142.2 %all-gather.2.cloned.1.call-start = ((), (), s32[]{:S(2)}) async-start(), calls=%async_computation.5 | async-start | bytes 15728640 | tf_op jit(solution)/shard_map/all_gather | solution.py:37
  14.1 0.7 copy-start.9
  14.1 1.1 copy-start.2
  17.2 44.0 %all-to-all-start = ((bf16[4,128,2048]{2,1,0:T(8,128)(2,1)}), bf16[4,128,2048]{2,1,0:T(8,128)(2,1)}, u32[]{:S(2)}, u32[]{:S(2)}) async-start(bf16[4,128,2048]{2,1,0:T(8,128)(2,1)} %broadcast_in_dim.8), calls=%async_computation | async-start | bytes 4194304 | tf_op jit(solution)/shard_map/all_to_all | solution.py:18
  34.5 40.5 %copy-start.6 = (bf16[512,512]{1,0:T(8,128)(2,1)S(1)}, bf16[512,512]{1,0:T(8,128)(2,1)}, u32[]{:S(2)}) copy-start(bf16[512,512]{1,0:T(8,128)(2,1)} %param.16) | copy-start | bytes 1572868
  34.5 40.5 %copy-start.7 = (bf16[512,512]{1,0:T(8,128)(2,1)S(1)}, bf16[512,512]{1,0:T(8,128)(2,1)}, u32[]{:S(2)}) copy-start(bf16[512,512]{1,0:T(8,128)(2,1)} %param.17) | copy-start | bytes 1572868
  34.5 42.9 %copy-start.8 = (bf16[3,512]{1,0:T(4,128)(2,1)S(1)}, bf16[3,512]{1,0:T(4,128)(2,1)}, u32[]{:S(2)}) copy-start(bf16[3,512]{1,0:T(4,128)(2,1)} %param.18) | copy-start | bytes 9220
  61.2 65.0 %all-to-all-start.1 = ((bf16[64,8,2048]{2,1,0:T(8,128)(2,1)}), bf16[64,8,2048]{2,1,0:T(8,128)(2,1)}, u32[]{:S(2)}, u32[]{:S(2)}) async-start(bf16[64,8,2048]{2,1,0:T(8,128)(2,1)} %bitcast_multiply_fusion), calls=%async_computation.2 | async-start | bytes 4194304 | tf_op jit(solution)/shard_map/all_to_all | solution.py:72
  75.0 127.7 %reduce-scatter.2.cloned.1.call-start = ((), (), s32[]{:S(2)}) async-start(), calls=%async_computation.4 | async-start | bytes 5242880 | tf_op jit(solution)/shard_map/reduce_scatter | solution.py:153
  75.1 5.8 %copy-start.12 = (bf16[512,512]{1,0:T(8,128)(2,1)S(1)}, bf16[512,512]{1,0:T(8,128)(2,1)}, u32[]{:S(2)}) copy-start(bf16[512,512]{1,0:T(8,128)(2,1)} %param.15) | copy-start | bytes 1572868
  75.1 5.5 %collective-permute-start = (bf16[2,2,512]{2,1,0:T(2,128)(2,1)S(1)}, bf16[2,2,512]{2,1,0:T(2,128)(2,1)S(1)}, u32[]{:S(2)}, u32[]{:S(2)}) collective-permute-start(bf16[2,2,512]{2,1,0:T(2,128)(2,1)S(1)} %pad_maximum_fusion.2), channel_id=1, source_target_pairs={{0,4},{4,8},{8,12},{12,16},{16,20},{20,24},{24,28},{28,32},{32,36}... | collective-permute-start | bytes 12296 | tf_op jit(solution)/shard_map/ppermute | solution.py:13
  80.9 2.8 %copy-start.10 = (bf16[2048,256]{1,0:T(8,128)(2,1)S(1)}, bf16[2048,256]{1,0:T(8,128)(2,1)}, u32[]{:S(2)}) copy-start(bf16[2048,256]{1,0:T(8,128)(2,1)} %param.25) | copy-start | bytes 3145732
  83.6 3.2 %copy-start.11 = (bf16[256,2048]{1,0:T(8,128)(2,1)S(1)}, bf16[256,2048]{1,0:T(8,128)(2,1)}, u32[]{:S(2)}) copy-start(bf16[256,2048]{1,0:T(8,128)(2,1)} %param.27) | copy-start | bytes 3145732
  86.9 5.8 %copy-start.3 = (bf16[512,2048]{1,0:T(8,128)(2,1)S(1)}, bf16[512,2048]{1,0:T(8,128)(2,1)}, u32[]{:S(2)}) copy-start(bf16[512,2048]{1,0:T(8,128)(2,1)} %convolution_convert_fusion.5) | copy-start | bytes 6291460
  149.4 6.4 %copy-start.4 = (bf16[1024,6144]{1,0:T(8,128)(2,1)S(1)}, bf16[1024,6144]{1,0:T(8,128)(2,1)}, u32[]{:S(2)}) copy-start(bf16[1024,6144]{1,0:T(8,128)(2,1)} %all-gather.2.cloned.1.call-done) | copy-start | bytes 37748740
  165.4 63.3 %all-to-all-start.2 = ((bf16[64,8,2048]{2,1,0:T(8,128)(2,1)}), bf16[64,8,2048]{2,1,0:T(8,128)(2,1)S(1)}, u32[]{:S(2)}, u32[]{:S(2)}) async-start(bf16[64,8,2048]{2,1,0:T(8,128)(2,1)} %fusion.2), calls=%async_computation.3 | async-start | bytes 4194304 | tf_op jit(solution)/shard_map/all_to_all | solution.py:163
  230.1 8.2 %copy-start.1 = (bf16[512,2048]{1,0:T(8,128)(2,1)S(1)}, bf16[512,2048]{1,0:T(8,128)(2,1)}, u32[]{:S(2)}) copy-start(bf16[512,2048]{1,0:T(8,128)(2,1)} %param.19) | copy-start | bytes 6291460
  232.4 4.9 %copy-start.5 = (bf16[256,2048]{1,0:T(8,128)(2,1)S(1)}, bf16[256,2048]{1,0:T(8,128)(2,1)}, u32[]{:S(2)}) copy-start(bf16[256,2048]{1,0:T(8,128)(2,1)} %reduce-scatter.2.cloned.1.call-done) | copy-start | bytes 3145732
Sparse Core Ops, SparseCore 0:
  14.3 135.0 all-gather.1
  151.9 50.6 reduce-scatter.1
where the time goes:
time: 246 us; the launch traced here: 245 us
  waiting for transfers between devices  131 us (53%)
  starting transfers between devices  32.8 us (13%)
  matrix products  26.1 us (11%)
  local copies, waits for them, and re-layouts  22.4 us (9%)
  other arithmetic  18.6 us (8%)
  between operations  14.3 us (6%)
    all_to_all x1, waiting for transfers between devices, send_own(): lax.all_to_all(outgoing, 'ep', split_axis=0, concat_axis=0, tiled=True)  29.3 us
    all_to_all x1, waiting for transfers between devices, from_everyone(): lax.all_to_all(jnp.broadcast_to(array[None], (length, *array.shape)), axi...  26.7 us
    reduce_scatter x1, waiting for transfers between devices, per_device(): lax.psum_scatter(combined.reshape(dev_count * joint_block, model_width).a...  24.4 us
    all_to_all x1, waiting for transfers between devices, per_device(): lax.all_to_all(routed_back, 'ep', split_axis=0, concat_axis=0, tiled=True)  24.2 us
    all_gather x1, waiting for transfers between devices, gather_turned(): result, at, outs = (lax.all_gather(both, axis, axis=0, tiled=True), 0, [])  23.3 us
    all_to_all x1, starting transfers between devices, send_own(): lax.all_to_all(outgoing, 'ep', split_axis=0, concat_axis=0, tiled=True)  13.8 us
    all_to_all x1, starting transfers between devices, per_device(): lax.all_to_all(routed_back, 'ep', split_axis=0, concat_axis=0, tiled=True)  12.1 us
    dot_general x2, matrix products, swiglu(): gate_term = jnp.dot(inputs, gate_w, preferred_element_type=jnp.float32)  8.57 us
  transfers between devices with their start and end apart: 6, of which 6 were waited for; matrix products, arithmetic and copies ran while one was open for 20% of the time, Pallas kernels for 0%

commit v1 on v0

--- a/solution.py
+++ b/solution.py
@@ -34,7 +34,13 @@
 def gather_turned(arrays, axis, dims):
     turned = [jnp.moveaxis(a, dim, 0) for a, dim in zip(arrays, dims)]
     both = jnp.concatenate([t.reshape(len(t), -1) for t in turned], axis=1)
-    result, at, outs = (lax.all_gather(both, axis, axis=0, tiled=True), 0, [])
+    save_run = lambda arr_in, axis_id: jnp.concatenate(
+        lax.all_to_all(
+            jnp.stack([arr_in for _ in range(lax.psum(1, axis_id))], axis=0), axis_id, 0, 0
+        ),
+        axis=0,
+    )
+    result, at, outs = (save_run(both, axis), 0, [])
     for t, dim in zip(turned, dims):
         share = result[:, at : at + t[0].size].reshape(-1, *t.shape[1:])
         outs.append(jnp.moveaxis(share, 0, dim))

time: 246 us -> 385 us (1.57)
  waiting for transfers between devices: 131 us -> 260 us
  local copies, waits for them, and re-layouts: 22.4 us -> 30.1 us
    all_to_all x0 -> x1, waiting for transfers between devices: none -> 150 us  [gather_turned(): lax.all_to_all(jnp.stack([arr_in for _ in range(lax.psum(1, axis_id))], a...]
    reduce_scatter x1, waiting for transfers between devices: 24.4 us -> 0.02 us  [per_device(): lax.psum_scatter(combined.reshape(dev_count * joint_block, model_width).a...]
    all_to_all x1, waiting for transfers between devices: 24.2 us -> 48.5 us  [per_device(): lax.all_to_all(routed_back, 'ep', split_axis=0, concat_axis=0, tiled=True)]
    all_gather x1 -> x0, waiting for transfers between devices: 23.3 us -> none  [gather_turned(): result, at, outs = (lax.all_gather(both, axis, axis=0, tiled=True), 0, [])]
    all_to_all x1, waiting for transfers between devices: 29.3 us -> 44.4 us  [send_own(): lax.all_to_all(outgoing, 'ep', split_axis=0, concat_axis=0, tiled=True)]
    all_to_all x1, waiting for transfers between devices: 26.7 us -> 14.3 us  [from_everyone(): lax.all_to_all(jnp.broadcast_to(array[None], (length, *array.shape)), axi...]
    another operation x1 -> x2, local copies, waits for them, and re-layouts: 0.01 us -> 7.94 us  [the longest x1 7.93 us: gather_turned(): jnp.stack([arr_in for _ in range(lax.psum(1, axis_id))], axis=0)]
    all_to_all x0 -> x1, starting transfers between devices: none -> 6.46 us  [gather_turned(): lax.all_to_all(jnp.stack([arr_in for _ in range(lax.psum(1, axis_id))], a...]
  transfers between devices with their start and end apart: 6 -> 6, of which waited for: 6 -> 5; matrix products, arithmetic and copies ran while one was open for 20% -> 14% of each run, Pallas kernels for 0% -> 0%
where the time goes in v1:
time: 385 us
  waiting for transfers between devices  260 us (68%)
  starting transfers between devices  32.4 us (8%)
  local copies, waits for them, and re-layouts  30.1 us (8%)
  matrix products  26.9 us (7%)
  other arithmetic  21.1 us (5%)
  between operations  14.3 us (4%)
    all_to_all x1, waiting for transfers between devices, gather_turned(): lax.all_to_all(jnp.stack([arr_in for _ in range(lax.psum(1, axis_id))], a...  150 us
    all_to_all x1, waiting for transfers between devices, per_device(): lax.all_to_all(routed_back, 'ep', split_axis=0, concat_axis=0, tiled=True)  48.5 us
    all_to_all x1, waiting for transfers between devices, send_own(): lax.all_to_all(outgoing, 'ep', split_axis=0, concat_axis=0, tiled=True)  44.4 us
    all_to_all x1, waiting for transfers between devices, from_everyone(): lax.all_to_all(jnp.broadcast_to(array[None], (length, *array.shape)), axi...  14.3 us
    all_to_all x1, starting transfers between devices, send_own(): lax.all_to_all(outgoing, 'ep', split_axis=0, concat_axis=0, tiled=True)  12.3 us
    dot_general x2, matrix products, swiglu(): gate_term = jnp.dot(inputs, gate_w, preferred_element_type=jnp.float32)  8.38 us
    another operation x1, local copies, waits for them, and re-layouts, gather_turned(): jnp.stack([arr_in for _ in range(lax.psum(1, axis_id))], axis=0)  7.93 us
  transfers between devices with their start and end apart: 6, of which 5 were waited for; matrix products, arithmetic and copies ran while one was open for 14% of the time, Pallas kernels for 0%

profile of v1, /device:TPU:8, one launch (start us, length us, event | category | flops | bytes accessed | tf_op | source)
XLA Modules:
  0.0 384.6 jit_solution(6951593752219085917)
XLA Ops:
  7.2 0.0 copy-start
  7.2 0.8 convert_element_type.85
  8.0 1.2 fusion.8
  9.3 1.2 fusion.10
  10.5 1.6 broadcast_in_dim.8
  12.1 4.5 %all-to-all-start = ((bf16[4,128,2048]{2,1,0:T(8,128)(2,1)}), bf16[4,128,2048]{2,1,0:T(8,128)(2,1)}, u32[]{:S(2)}, u32[]{:S(2)}) async-start(bf16[4,128,2048]{2,1,0:T(8,128)(2,1)} %broadcast_in_dim.8), calls=%async_computation | async-start | bytes 4194304 | tf_op jit(solution)/shard_map/all_to_all | solution.py:18
  16.6 0.7 broadcast_multiply_fusion
  17.3 0.1 copy.21
  17.4 0.1 eq.25
  17.6 0.1 eq.29
  17.7 0.1 copy.20
  17.8 0.1 mul.132
  18.0 0.6 reduce-window.6
  18.6 0.2 slice_reduce_fusion
  18.8 0.1 fusion.31
  18.9 1.4 scatter_custom_fusion
  20.4 3.3 gather_fusion
  23.7 2.2 scatter_custom_fusion.1
  25.8 0.1 mul.134
  25.9 3.1 bitcast_multiply_fusion
  29.0 14.3 %all-to-all-done = bf16[4,128,2048]{2,1,0:T(8,128)(2,1)} async-done(((bf16[4,128,2048]{2,1,0:T(8,128)(2,1)}), bf16[4,128,2048]{2,1,0:T(8,128)(2,1)}, u32[]{:S(2)}, u32[]{:S(2)}) %all-to-all-start) | async-done | bytes 2097184 | tf_op jit(solution)/shard_map/all_to_all | solution.py:18
  43.3 12.3 %all-to-all-start.1 = ((bf16[64,8,2048]{2,1,0:T(8,128)(2,1)}), bf16[64,8,2048]{2,1,0:T(8,128)(2,1)}, u32[]{:S(2)}, u32[]{:S(2)}) async-start(bf16[64,8,2048]{2,1,0:T(8,128)(2,1)} %bitcast_multiply_fusion), calls=%async_computation.2 | async-start | bytes 4194304 | tf_op jit(solution)/shard_map/all_to_all | solution.py:78
  55.6 1.5 copy.25
  57.1 2.3 copy.24
  59.4 3.0 pad_maximum_fusion.1
  62.4 44.4 %all-to-all-done.1 = bf16[64,8,2048]{2,1,0:T(8,128)(2,1)} async-done(((bf16[64,8,2048]{2,1,0:T(8,128)(2,1)}), bf16[64,8,2048]{2,1,0:T(8,128)(2,1)}, u32[]{:S(2)}, u32[]{:S(2)}) %all-to-all-start.1) | async-done | bytes 2097184 | tf_op jit(solution)/shard_map/all_to_all | solution.py:78
  106.7 7.9 %stack.19 = bf16[4,256,6144]{2,1,0:T(8,128)(2,1)} broadcast(bf16[256,6144]{1,0:T(8,128)(2,1)} %pad_maximum_fusion.1), dimensions={1,2} | broadcast | bytes 15728640 | tf_op jit(solution)/shard_map/stack | solution.py:39
  114.7 6.5 %all-to-all-start.2 = ((bf16[4,256,6144]{2,1,0:T(8,128)(2,1)}), bf16[4,256,6144]{2,1,0:T(8,128)(2,1)}, u32[]{:S(2)}, u32[]{:S(2)}) async-start(bf16[4,256,6144]{2,1,0:T(8,128)(2,1)} %stack.19), calls=%async_computation.3 | async-start | bytes 25165824 | tf_op jit(solution)/shard_map/all_to_all | solution.py:38
  121.1 0.0 reduce-scatter.2.cloned.1.call-start
  121.2 0.0 copy-done.4
  121.2 0.0 copy-done.5
  121.2 0.0 copy-start.9
  121.3 2.2 collective-permute-start
  123.5 0.0 copy-done.6
  123.5 2.8 collective-permute-done
  126.3 0.2 convert_multiply_fusion.2
  126.6 0.0 copy-done
  126.6 0.0 copy-done.9
  126.6 0.0 copy-start.7
  126.6 2.7 convolution_convert_fusion.5
  129.3 3.2 fusion.39
  132.5 0.0 copy-done.8
  132.5 5.8 %convolution_convert_fusion.4 = bf16[512,2048]{1,0:T(8,128)(2,1)} fusion(bf16[256,2048]{1,0:T(8,128)(2,1)S(1)} %copy-done.8, bf16[512,2048]{1,0:T(8,128)(2,1)} %bitcast.8, bf16[2048,256]{1,0:T(8,128)(2,1)} %param.26, f32[512,256]{1,0:T(8,128)} %fusion.39), kind=kOutput, calls=%fused_computation.16 | convolution fusion | flops 1075576832 | bytes 6815744 | tf_op jit(solution)/shard_map/dot_general | solution.py:152
  138.3 4.1 %pad_maximum_fusion = bf16[4,256,2048]{2,1,0:T(8,128)(2,1)} fusion(bf16[4,128,2048]{2,1,0:T(8,128)(2,1)} %bitcast.97, bf16[4,128,2048]{2,1,0:T(8,128)(2,1)S(1)} %bitcast.96), kind=kLoop, calls=%fused_computation.9 | loop fusion | flops 8388608 | bytes 8388608 | tf_op jit(solution)/shard_map/concatenate | solution.py:156
  142.5 0.0 reduce-scatter.2.cloned.1.call-update
  142.5 149.9 %all-to-all-done.2 = bf16[4,256,6144]{2,1,0:T(8,128)(2,1)} async-done(((bf16[4,256,6144]{2,1,0:T(8,128)(2,1)}), bf16[4,256,6144]{2,1,0:T(8,128)(2,1)}, u32[]{:S(2)}, u32[]{:S(2)}) %all-to-all-start.2) | async-done | bytes 12582944 | tf_op jit(solution)/shard_map/all_to_all | solution.py:38
  292.4 5.2 %fusion.1 = f32[512,1024]{1,0:T(8,128)S(1)} fusion(bf16[1024,6144]{1,0:T(8,128)(2,1)} %bitcast.21, bf16[64,8,2048]{2,1,0:T(8,128)(2,1)} %all-to-all-done.1), kind=kOutput, calls=%fused_computation.8 | convolution fusion | flops 2147483648 | bytes 8388608 | tf_op jit(solution)/shard_map/dot_general | solution.py:58
  297.5 2.5 slice_bitcast_fusion
  300.0 5.3 %multiply_convert_fusion = bf16[512,1024]{1,0:T(8,128)(2,1)S(1)} fusion(f32[512,1024]{1,0:T(8,128)S(1)} %fusion.1, bf16[1024,6144]{1,0:T(8,128)(2,1)} %bitcast.21, bf16[64,8,2048]{2,1,0:T(8,128)(2,1)} %all-to-all-done.1), kind=kOutput, calls=%fused_computation.23 | convolution fusion | flops 2150629376 | bytes 9437184 | tf_op jit(solution)/shard_map/dot_general | solution.py:59
  305.4 0.7 convolution_convert_fusion
  306.1 0.7 convolution_convert_fusion.1
  306.8 0.7 convolution_convert_fusion.2
  307.5 2.6 fusion.2
  310.1 6.8 %all-to-all-start.3 = ((bf16[64,8,2048]{2,1,0:T(8,128)(2,1)}), bf16[64,8,2048]{2,1,0:T(8,128)(2,1)S(1)}, u32[]{:S(2)}, u32[]{:S(2)}) async-start(bf16[64,8,2048]{2,1,0:T(8,128)(2,1)} %fusion.2), calls=%async_computation.4 | async-start | bytes 4194304 | tf_op jit(solution)/shard_map/all_to_all | solution.py:169
  317.0 0.7 constant_dynamic-slice_fusion
  317.7 0.1 copy.26
  317.8 0.0 reduce-scatter.2.cloned.1.call-done
  317.8 1.9 slice.117
  319.7 48.5 %all-to-all-done.3 = bf16[64,8,2048]{2,1,0:T(8,128)(2,1)S(1)} async-done(((bf16[64,8,2048]{2,1,0:T(8,128)(2,1)}), bf16[64,8,2048]{2,1,0:T(8,128)(2,1)S(1)}, u32[]{:S(2)}, u32[]{:S(2)}) %all-to-all-start.3) | async-done | bytes 2097184 | tf_op jit(solution)/shard_map/all_to_all | solution.py:169
  368.2 1.4 gather_fusion.1
  369.6 0.0 copy-start.1
  369.6 2.4 reshape.119
  372.0 4.9 %multiply_reduce_fusion = f32[128,2048]{1,0:T(8,128)S(1)} fusion(f32[128,2,2048]{2,1,0:T(2,128)} %reshape.119, f32[128,2]{1,0:T(8,128)S(1)} %copy.26), kind=kLoop, calls=%fused_computation.22 | loop fusion | flops 786432 | bytes 3146752 | tf_op jit(solution)/shard_map/reduce_sum | solution.py:173
  376.9 0.9 add_convert_fusion.1
  (24 shorter events, 0.1 us)
Async XLA Ops:
  7.2 119.4 %copy-start = (bf16[512,2048]{1,0:T(8,128)(2,1)S(1)}, bf16[512,2048]{1,0:T(8,128)(2,1)}, u32[]{:S(2)}) copy-start(bf16[512,2048]{1,0:T(8,128)(2,1)} %param.19) | copy-start | bytes 6291460
  12.1 31.2 %all-to-all-start = ((bf16[4,128,2048]{2,1,0:T(8,128)(2,1)}), bf16[4,128,2048]{2,1,0:T(8,128)(2,1)}, u32[]{:S(2)}, u32[]{:S(2)}) async-start(bf16[4,128,2048]{2,1,0:T(8,128)(2,1)} %broadcast_in_dim.8), calls=%async_computation | async-start | bytes 4194304 | tf_op jit(solution)/shard_map/all_to_all | solution.py:18
  43.3 63.5 %all-to-all-start.1 = ((bf16[64,8,2048]{2,1,0:T(8,128)(2,1)}), bf16[64,8,2048]{2,1,0:T(8,128)(2,1)}, u32[]{:S(2)}, u32[]{:S(2)}) async-start(bf16[64,8,2048]{2,1,0:T(8,128)(2,1)} %bitcast_multiply_fusion), calls=%async_computation.2 | async-start | bytes 4194304 | tf_op jit(solution)/shard_map/all_to_all | solution.py:78
  114.7 6.5 %copy-start.4 = (bf16[512,512]{1,0:T(8,128)(2,1)S(1)}, bf16[512,512]{1,0:T(8,128)(2,1)}, u32[]{:S(2)}) copy-start(bf16[512,512]{1,0:T(8,128)(2,1)} %param.16) | copy-start | bytes 1572868
  114.7 6.5 %copy-start.5 = (bf16[512,512]{1,0:T(8,128)(2,1)S(1)}, bf16[512,512]{1,0:T(8,128)(2,1)}, u32[]{:S(2)}) copy-start(bf16[512,512]{1,0:T(8,128)(2,1)} %param.17) | copy-start | bytes 1572868
  114.7 8.8 %copy-start.6 = (bf16[3,512]{1,0:T(4,128)(2,1)S(1)}, bf16[3,512]{1,0:T(4,128)(2,1)}, u32[]{:S(2)}) copy-start(bf16[3,512]{1,0:T(4,128)(2,1)} %param.18) | copy-start | bytes 9220
  114.7 177.7 %all-to-all-start.2 = ((bf16[4,256,6144]{2,1,0:T(8,128)(2,1)}), bf16[4,256,6144]{2,1,0:T(8,128)(2,1)}, u32[]{:S(2)}, u32[]{:S(2)}) async-start(bf16[4,256,6144]{2,1,0:T(8,128)(2,1)} %stack.19), calls=%async_computation.3 | async-start | bytes 25165824 | tf_op jit(solution)/shard_map/all_to_all | solution.py:38
  121.1 196.7 %reduce-scatter.2.cloned.1.call-start = ((), (), s32[]{:S(2)}) async-start(), calls=%async_computation.5 | async-start | bytes 5242880 | tf_op jit(solution)/shard_map/reduce_scatter | solution.py:159
  121.2 5.4 %copy-start.9 = (bf16[512,512]{1,0:T(8,128)(2,1)S(1)}, bf16[512,512]{1,0:T(8,128)(2,1)}, u32[]{:S(2)}) copy-start(bf16[512,512]{1,0:T(8,128)(2,1)} %param.15) | copy-start | bytes 1572868
  121.3 5.1 %collective-permute-start = (bf16[2,2,512]{2,1,0:T(2,128)(2,1)S(1)}, bf16[2,2,512]{2,1,0:T(2,128)(2,1)S(1)}, u32[]{:S(2)}, u32[]{:S(2)}) collective-permute-start(bf16[2,2,512]{2,1,0:T(2,128)(2,1)S(1)} %pad_maximum_fusion.2), channel_id=1, source_target_pairs={{0,4},{4,8},{8,12},{12,16},{16,20},{20,24},{24,28},{28,32},{32,36}... | collective-permute-start | bytes 12296 | tf_op jit(solution)/shard_map/ppermute | solution.py:13
  126.6 2.7 copy-start.7
  129.3 3.2 copy-start.8
  132.5 5.8 %copy-start.2 = (bf16[512,2048]{1,0:T(8,128)(2,1)S(1)}, bf16[512,2048]{1,0:T(8,128)(2,1)}, u32[]{:S(2)}) copy-start(bf16[512,2048]{1,0:T(8,128)(2,1)} %convolution_convert_fusion.5) | copy-start | bytes 6291460
  310.1 58.1 %all-to-all-start.3 = ((bf16[64,8,2048]{2,1,0:T(8,128)(2,1)}), bf16[64,8,2048]{2,1,0:T(8,128)(2,1)S(1)}, u32[]{:S(2)}, u32[]{:S(2)}) async-start(bf16[64,8,2048]{2,1,0:T(8,128)(2,1)} %fusion.2), calls=%async_computation.4 | async-start | bytes 4194304 | tf_op jit(solution)/shard_map/all_to_all | solution.py:169
  369.6 8.2 %copy-start.1 = (bf16[512,2048]{1,0:T(8,128)(2,1)S(1)}, bf16[512,2048]{1,0:T(8,128)(2,1)}, u32[]{:S(2)}) copy-start(bf16[512,2048]{1,0:T(8,128)(2,1)} %param.19) | copy-start | bytes 6291460
  372.0 4.9 %copy-start.3 = (bf16[256,2048]{1,0:T(8,128)(2,1)S(1)}, bf16[256,2048]{1,0:T(8,128)(2,1)}, u32[]{:S(2)}) copy-start(bf16[256,2048]{1,0:T(8,128)(2,1)} %reduce-scatter.2.cloned.1.call-done) | copy-start | bytes 3145732
Sparse Core Ops, SparseCore 0:
  142.6 81.4 reduce-scatter.1
